TPU v7x, 128 devices: a whole 4x4x4 slice. The times are simulated.
128 devices in a mesh: fs: 16 (over z, y), tp: 8 (over x, core).
Axes of the slice: x: 4, y: 4, z: 4, core: 2. Of those that a mesh axis runs over, the one named last changes fastest.
Arguments:
- tokens: bfloat16 [16384, 2048], P(('fs', 'tp')), may hold values from -6 to 6
- first_block_norm_scale: float32 [2048], replicated, may hold values from 0.1 to 1.9
- first_block_gate_matrix: bfloat16 [2048, 5504], P('fs', 'tp'), may hold values from -0.125 to 0.125
- first_block_up_matrix: bfloat16 [2048, 5504], P('fs', 'tp'), may hold values from -0.125 to 0.125
- first_block_down_matrix: bfloat16 [5504, 2048], P('tp', 'fs'), may hold values from -0.078125 to 0.078125
- mixer_norm_scale: float32 [2048], replicated, may hold values from 0.1 to 1.9
- recurrent_input_matrix: bfloat16 [2048, 3072], P('fs', 'tp'), may hold values from -0.125 to 0.125
- output_gate_projection: bfloat16 [2048, 3072], P('fs', 'tp'), may hold values from -0.125 to 0.125
- convolution_kernel: float32 [4, 3072], P(None, 'tp'), may hold values from -2 to 2
- decay_gate_blocks: bfloat16 [16, 192, 192], P('tp'), may hold values from -0.4375 to 0.4375
- input_gate_blocks: bfloat16 [16, 192, 192], P('tp'), may hold values from -0.4375 to 0.4375
- channel_decay_weight: float32 [3072], P('tp'), may hold values from 3.5 to 11.5
- position_decay_extra: float32 [16384], P('fs'), may hold values from -0.7 to 0
- mixer_output_matrix: bfloat16 [3072, 2048], P('tp', 'fs'), may hold values from -0.109375 to 0.109375
- second_block_norm_scale: float32 [2048], replicated, may hold values from 0.1 to 1.9
- second_block_gate_matrix: bfloat16 [2048, 5504], P('fs', 'tp'), may hold values from -0.125 to 0.125
- second_block_up_matrix: bfloat16 [2048, 5504], P('fs', 'tp'), may hold values from -0.125 to 0.125
- second_block_down_matrix: bfloat16 [5504, 2048], P('tp', 'fs'), may hold values from -0.078125 to 0.078125
Outputs:
- layer_out: bfloat16 [16384, 2048], P(('fs', 'tp'))
All inputs are finite; a program needn't handle non-finite values.
Results may differ from a plain program's by a relative error of at most 0.019.
Values may be sent and summed in bfloat16 or wider, within the bound.
A program may use at most 128 MiB of HBM per device.

v0:
```python
import jax
import jax.numpy as jnp
from jax import lax
from jax.sharding import PartitionSpec as P

EPS = 1e-06
RECURRENT_WIDTH = 8.0


def in_one_piece(arrays, axis, dim, along):
    both = jnp.concatenate(arrays, axis=along)
    filled, at, gathered = (lax.all_gather(both, axis, axis=dim, tiled=True), 0, [])
    for a in arrays:
        gathered.append(lax.slice_in_dim(filled, at, at + a.shape[along], axis=along))
        at += a.shape[along]
    return tuple(gathered)


def copy_for_each(x, axis):
    copies = jnp.broadcast_to(x, (lax.axis_size(axis), *x.shape))
    return lax.all_to_all(copies, axis, split_axis=0, concat_axis=0, tiled=True)


def laid_out(tiles, dim):
    lengths = list(tiles.shape[1:])
    lengths[dim] *= tiles.shape[0]
    return jnp.moveaxis(tiles, 0, dim).reshape(lengths)


def gathered_copies(x, axis, dim):
    tiles = copy_for_each(x, axis)
    return laid_out(tiles, dim)


def cut_along(x, dim, devices):
    before, after = (x.shape[:dim], x.shape[dim + 1 :])
    return jnp.moveaxis(x.reshape(*before, devices, -1, *after), dim, 0)


def sent_and_summed(x, axis, dim):
    devices = lax.axis_size(axis)
    tiles = lax.all_to_all(cut_along(x, dim, devices), axis, 0, 0, tiled=True)
    return jnp.sum(tiles.astype(jnp.float32), axis=0)


def normed(input_token_rows, norm_scale_vector):
    values = input_token_rows.astype(jnp.float32)
    square = jnp.mean(values * values, axis=-1, keepdims=True)
    return (values * lax.rsqrt(square + EPS) * norm_scale_vector).astype(jnp.bfloat16)


def combine(earlier, later):
    decay_one, drive_one = earlier
    decay_two, drive_two = later
    return (decay_one * decay_two, decay_two * drive_one + drive_two)


def sublayer(
    residual_activations,
    norm_scale_vector,
    first_weight,
    second_weight,
    out_weight,
    middle,
    sequence,
    row_count,
):
    normal = normed(residual_activations, norm_scale_vector)
    full_first, full_second = in_one_piece((first_weight, second_weight), "fs", 0, 1)
    piece = lax.all_gather(normal, "tp", axis=0, tiled=True)
    projected = middle(
        jnp.dot(piece, full_first, preferred_element_type=jnp.float32),
        jnp.dot(piece, full_second, preferred_element_type=jnp.float32),
    )
    if sequence is not None:
        projected = sequence(projected)
    full_out = gathered_copies(out_weight, "fs", 1)
    picked = lax.slice_in_dim(projected, 0, row_count * lax.axis_size("tp"), axis=0)
    return sent_and_summed(
        jnp.dot(picked, full_out, preferred_element_type=jnp.float32).astype(jnp.bfloat16), "tp", 0
    )


def shards(
    tokens,
    first_block_norm_scale,
    first_block_gate_matrix,
    first_block_up_matrix,
    first_block_down_matrix,
    mixer_norm_scale,
    recurrent_input_matrix,
    output_gate_projection,
    convolution_kernel,
    decay_gate_blocks,
    input_gate_blocks,
    channel_decay_weight,
    position_decay_extra,
    mixer_output_matrix,
    second_block_norm_scale,
    second_block_gate_matrix,
    second_block_up_matrix,
    second_block_down_matrix,
):
    row_count = tokens.shape[0]
    residual_activations = tokens

    def feed_middle(gate_pre, up_pre):
        return (jax.nn.silu(gate_pre) * up_pre).astype(jnp.bfloat16)

    def mixer_middle(recur_pre, branch_pre):
        return jnp.concatenate(
            [recur_pre.astype(jnp.bfloat16), branch_pre.astype(jnp.bfloat16)], axis=1
        )

    def recurrent(projected):
        channels = projected.shape[1] // 2
        length = projected.shape[0]
        recur_rows = projected[:, :channels]
        branch_rows = projected[:, channels:]
        taps = convolution_kernel.shape[0]
        summed = lax.conv_general_dilated(
            recur_rows.astype(jnp.float32)[None],
            convolution_kernel[:, None, :],
            window_strides=(1,),
            padding=((taps - 1, 0),),
            dimension_numbers=("NWC", "WIO", "NWC"),
            feature_group_count=channels,
            precision=lax.Precision.HIGHEST,
        )[0]
        conv_out = summed.astype(jnp.bfloat16)
        grouped = conv_out.reshape(length, decay_gate_blocks.shape[0], decay_gate_blocks.shape[1])
        decay_gate_value = jax.nn.sigmoid(
            jnp.einsum(
                "thi,hij->thj", grouped, decay_gate_blocks, preferred_element_type=jnp.float32
            ).reshape(length, channels)
        )
        input_gate = jax.nn.sigmoid(
            jnp.einsum(
                "thi,hij->thj", grouped, input_gate_blocks, preferred_element_type=jnp.float32
            ).reshape(length, channels)
        )
        log_decay_factor = (
            -RECURRENT_WIDTH * decay_gate_value * jax.nn.softplus(-channel_decay_weight)
            + position_decay_extra[:, None]
        )
        decay_rate = jnp.exp(log_decay_factor)
        drive_in = (
            jnp.sqrt(-jnp.expm1(2.0 * log_decay_factor)) * input_gate * conv_out.astype(jnp.float32)
        )
        _, hidden_state = lax.associative_scan(combine, (decay_rate, drive_in), axis=0)
        return (
            jax.nn.gelu(branch_rows.astype(jnp.float32), approximate=True) * hidden_state
        ).astype(jnp.bfloat16)

    first_out = sublayer(
        residual_activations,
        first_block_norm_scale,
        first_block_gate_matrix,
        first_block_up_matrix,
        first_block_down_matrix,
        feed_middle,
        None,
        row_count,
    )
    residual_activations = (residual_activations.astype(jnp.float32) + 0.5 * first_out).astype(
        jnp.bfloat16
    )
    mixer_output_rows = sublayer(
        residual_activations,
        mixer_norm_scale,
        recurrent_input_matrix,
        output_gate_projection,
        mixer_output_matrix,
        mixer_middle,
        recurrent,
        row_count,
    )
    residual_activations = (residual_activations.astype(jnp.float32) + mixer_output_rows).astype(
        jnp.bfloat16
    )
    second_out = sublayer(
        residual_activations,
        second_block_norm_scale,
        second_block_gate_matrix,
        second_block_up_matrix,
        second_block_down_matrix,
        feed_middle,
        None,
        row_count,
    )
    residual_activations = (residual_activations.astype(jnp.float32) + 0.5 * second_out).astype(
        jnp.bfloat16
    )
    return residual_activations


def solution(mesh):
    in_specs = (
        P(("fs", "tp"), None),
        P(),
        P("fs", "tp"),
        P("fs", "tp"),
        P("tp", "fs"),
        P(),
        P("fs", "tp"),
        P("fs", "tp"),
        P(None, "tp"),
        P("tp", None, None),
        P("tp", None, None),
        P("tp"),
        P("fs"),
        P("tp", "fs"),
        P(),
        P("fs", "tp"),
        P("fs", "tp"),
        P("tp", "fs"),
    )
    out_specs = P(("fs", "tp"), None)
    return jax.shard_map(shards, mesh=mesh, in_specs=in_specs, out_specs=out_specs, check_vma=False)
```

profile of v0, /device:TPU:1, one launch (start us, length us, event | category | flops | bytes accessed | tf_op | source)
XLA Modules:
  0.0 540.3 jit_solution(13397318217952377570)
XLA Ops:
  7.8 2.0 fusion.40
  9.9 1.8 pad_maximum_fusion.2
  11.7 2.0 broadcast_in_dim.10
  13.7 8.7 %all-to-all-start = ((bf16[16,688,128]{2,1,0:T(8,128)(2,1)}), bf16[16,688,128]{2,1,0:T(8,128)(2,1)S(1)}, u32[]{:S(2)}, u32[]{:S(2)}) async-start(bf16[16,688,128]{2,1,0:T(8,128)(2,1)} %broadcast_in_dim.10), calls=%async_computation | async-start | bytes 5636096 | tf_op jit(solution)/shard_map/all_to_all | solution.py:21
  23.3 22.4 %all-gather.7.cloned.1.call-done = bf16[1024,2048]{1,0:T(8,128)(2,1)} async-done(((bf16[128,2048]{1,0:T(8,128)(2,1)}), bf16[1024,2048]{1,0:T(8,128)(2,1)}) %all-gather.7.cloned.1.call-update) | async-done | bytes 4194320 | tf_op jit(solution)/shard_map/all_gather | solution.py:70
  45.7 65.6 %all-gather.9.cloned.1.call-done = bf16[2048,1376]{0,1:T(8,128)(2,1)} async-done(((bf16[128,1376]{0,1:T(8,128)(2,1)}), bf16[2048,1376]{0,1:T(8,128)(2,1)}) %all-gather.9.cloned.1.call-update) | async-done | bytes 5636112 | tf_op jit(solution)/shard_map/all_gather | solution.py:12
  111.2 7.7 %fusion.10 = f32[1024,688]{0,1:T(8,128)} fusion(bf16[1024,2048]{1,0:T(8,128)(2,1)} %all-gather.7.cloned.1.call-done, bf16[2048,1376]{0,1:T(8,128)(2,1)} %all-gather.9.cloned.1.call-done), kind=kOutput, calls=%fused_computation.16 | convolution fusion | flops 2885681152 | bytes 9830400 | tf_op jit(solution)/shard_map/dot_general | solution.py:72
  118.9 11.0 %convolution_convert_fusion.2 = bf16[1024,2048]{1,0:T(8,128)(2,1)} fusion(f32[1024,688]{0,1:T(8,128)} %fusion.10, bf16[1024,2048]{1,0:T(8,128)(2,1)} %all-gather.7.cloned.1.call-done, bf16[2048,1376]{0,1:T(8,128)(2,1)} %all-gather.9.cloned.1.call-done, bf16[16,688,128]{2,1,0:T(8,128)(2,1)S(1)} %all-to-all-done), kind=kOutput, calls=%fused_computation.5 | convolution fusion | flops 5777686528 | bytes 16842752 | tf_op jit(solution)/shard_map/dot_general | solution.py:80
  130.0 54.9 %all_to_all.30 = bf16[8,128,2048]{2,1,0:T(8,128)(2,1)S(1)} all-to-all(bf16[8,128,2048]{2,1,0:T(8,128)(2,1)} %bitcast.50), channel_id=1, replica_groups=mesh['fs'=16,'tp'=8] {'tp'}, dimensions={0} | all-to-all | bytes 8388608 | tf_op jit(solution)/shard_map/all_to_all | solution.py:42
  189.6 4.7 all-to-all-start.2
  195.4 23.0 %all-gather.11.cloned.1.call-done = bf16[1024,2048]{1,0:T(8,128)(2,1)} async-done(((bf16[128,2048]{1,0:T(8,128)(2,1)}), bf16[1024,2048]{1,0:T(8,128)(2,1)}) %all-gather.11.cloned.1.call-update) | async-done | bytes 4194320 | tf_op jit(solution)/shard_map/all_gather | solution.py:70
  218.4 5.0 fusion.35
  227.1 1.7 copy.46
  229.5 1.6 copy.48
  231.1 3.4 fusion.34
  234.6 2.8 slice.256
  237.4 2.8 slice.257
  240.2 2.8 slice.255
  242.9 2.8 slice.259
  245.7 3.2 fusion.89
  248.8 3.0 slice.262
  251.9 3.1 slice.263
  254.9 3.1 slice.261
  258.0 3.1 slice.265
  261.1 2.3 fusion.90
  263.4 1.7 slice.268
  265.1 1.7 slice.269
  266.8 1.7 slice.267
  268.5 1.7 slice.271
  274.1 1.7 fusion.92
  275.9 1.5 slice.280
  281.9 1.5 fusion.93
  316.9 1.5 slice.278
  324.3 1.7 slice.323
  327.3 3.1 slice.260
  330.4 3.1 slice.325
  334.8 2.8 slice.327
  337.6 2.8 slice.254
  346.6 3.1 pad.80
  351.3 10.3 %convolution_convert_fusion = bf16[1024,2048]{1,0:T(8,128)(2,1)} fusion(bf16[384,2048]{0,1:T(8,128)(2,1)} %bitcast.12, f32[1024,384]{1,0:T(8,128)S(1)} %pad.79, f32[1024,384]{1,0:T(8,128)} %pad.80, bf16[1024,2048]{1,0:T(8,128)(2,1)} %all-gather.11.cloned.1.call-done, bf16[2048,768]{1,0:T(8,128)(2,1)} %all-gather.13.cloned.1.call-done), kind=kOutput, calls=%fused_computation.3 | convolution fusion | flops 3228434432 | bytes 14680064 | tf_op jit(solution)/shard_map/dot_general | solution.py:80
  361.6 52.5 %all_to_all.31 = bf16[8,128,2048]{2,1,0:T(8,128)(2,1)S(1)} all-to-all(bf16[8,128,2048]{2,1,0:T(8,128)(2,1)} %bitcast.49), channel_id=1, replica_groups=mesh['fs'=16,'tp'=8] {'tp'}, dimensions={0} | all-to-all | bytes 8388608 | tf_op jit(solution)/shard_map/all_to_all | solution.py:42
  416.5 2.0 broadcast_in_dim.27
  418.5 6.7 %all-to-all-start.4 = ((bf16[16,688,128]{2,1,0:T(8,128)(2,1)}), bf16[16,688,128]{2,1,0:T(8,128)(2,1)S(1)}, u32[]{:S(2)}, u32[]{:S(2)}) async-start(bf16[16,688,128]{2,1,0:T(8,128)(2,1)} %broadcast_in_dim.27), calls=%async_computation.4 | async-start | bytes 5636096 | tf_op jit(solution)/shard_map/all_to_all | solution.py:21
  425.3 23.6 %all-gather.15.cloned.1.call-done = bf16[1024,2048]{1,0:T(8,128)(2,1)} async-done(((bf16[128,2048]{1,0:T(8,128)(2,1)}), bf16[1024,2048]{1,0:T(8,128)(2,1)}) %all-gather.15.cloned.1.call-update) | async-done | bytes 4194320 | tf_op jit(solution)/shard_map/all_gather | solution.py:70
  448.9 7.7 %fusion.6 = f32[1024,688]{0,1:T(8,128)} fusion(bf16[1024,2048]{1,0:T(8,128)(2,1)} %all-gather.15.cloned.1.call-done, bf16[2048,1376]{0,1:T(8,128)(2,1)} %all-gather.17.cloned.1.call-done), kind=kOutput, calls=%fused_computation.12 | convolution fusion | flops 2885681152 | bytes 9830400 | tf_op jit(solution)/shard_map/dot_general | solution.py:72
  456.6 9.6 %all-to-all-done.4 = bf16[16,688,128]{2,1,0:T(8,128)(2,1)S(1)} async-done(((bf16[16,688,128]{2,1,0:T(8,128)(2,1)}), bf16[16,688,128]{2,1,0:T(8,128)(2,1)S(1)}, u32[]{:S(2)}, u32[]{:S(2)}) %all-to-all-start.4) | async-done | bytes 2818080 | tf_op jit(solution)/shard_map/all_to_all | solution.py:21
  466.2 11.0 %convolution_convert_fusion.1 = bf16[1024,2048]{1,0:T(8,128)(2,1)} fusion(f32[1024,688]{0,1:T(8,128)} %fusion.6, bf16[1024,2048]{1,0:T(8,128)(2,1)} %all-gather.15.cloned.1.call-done, bf16[2048,1376]{0,1:T(8,128)(2,1)} %all-gather.17.cloned.1.call-done, bf16[16,688,128]{2,1,0:T(8,128)(2,1)S(1)} %all-to-all-done.4), kind=kOutput, calls=%fused_computation.4 | convolution fusion | flops 5777686528 | bytes 16842752 | tf_op jit(solution)/shard_map/dot_general | solution.py:80
  477.3 54.5 %all_to_all.32 = bf16[8,128,2048]{2,1,0:T(8,128)(2,1)S(1)} all-to-all(bf16[8,128,2048]{2,1,0:T(8,128)(2,1)} %bitcast.51), channel_id=1, replica_groups=mesh['fs'=16,'tp'=8] {'tp'}, dimensions={0} | all-to-all | bytes 8388608 | tf_op jit(solution)/shard_map/all_to_all | solution.py:42
  (213 shorter events, 73.6 us)
Async XLA Ops:
  6.5 219.9 %copy-start = (bf16[2,192,192]{2,1,0:T(8,128)(2,1)S(1)}, bf16[2,192,192]{2,1,0:T(8,128)(2,1)}, u32[]{:S(2)}) copy-start(bf16[2,192,192]{2,1,0:T(8,128)(2,1)} %param.27) | copy-start | bytes 442372
  6.5 5.2 copy-start.10
  6.5 39.1 %all-gather.7.cloned.1.call-start = ((), (), s32[]{:S(2)}) async-start(), calls=%async_computation.6 | async-start | bytes 4718592 | tf_op jit(solution)/shard_map/all_gather | solution.py:70
  9.9 101.4 %all-gather.9.cloned.1.call-start = ((), (), s32[]{:S(2)}) async-start(), calls=%async_computation.7 | async-start | bytes 5988352 | tf_op jit(solution)/shard_map/all_gather | solution.py:12
  13.7 8.8 %copy-start.15 = (bf16[128,384]{1,0:T(8,128)(2,1)S(1)}, bf16[128,384]{1,0:T(8,128)(2,1)}, u32[]{:S(2)}) copy-start(bf16[128,384]{1,0:T(8,128)(2,1)} %param.25) | copy-start | bytes 294916
  13.7 8.8 %copy-start.16 = (bf16[128,384]{1,0:T(8,128)(2,1)S(1)}, bf16[128,384]{1,0:T(8,128)(2,1)}, u32[]{:S(2)}) copy-start(bf16[128,384]{1,0:T(8,128)(2,1)} %param.24) | copy-start | bytes 294916
  13.7 105.2 %all-to-all-start = ((bf16[16,688,128]{2,1,0:T(8,128)(2,1)}), bf16[16,688,128]{2,1,0:T(8,128)(2,1)S(1)}, u32[]{:S(2)}, u32[]{:S(2)}) async-start(bf16[16,688,128]{2,1,0:T(8,128)(2,1)} %broadcast_in_dim.10), calls=%async_computation | async-start | bytes 5636096 | tf_op jit(solution)/shard_map/all_to_all | solution.py:21
  22.5 172.9 %all-gather.13.cloned.1.call-start = ((), (), s32[]{:S(2)}) async-start(), calls=%async_computation.9 | async-start | bytes 3342336 | tf_op jit(solution)/shard_map/all_gather | solution.py:12
  23.2 195.2 %all-gather.11.cloned.1.call-start = ((), (), s32[]{:S(2)}) async-start(), calls=%async_computation.8 | async-start | bytes 4718592 | tf_op jit(solution)/shard_map/all_gather | solution.py:70
  184.9 1.0 copy-start.3
  184.9 2.1 copy-start.25
  186.0 2.1 copy-start.14
  186.2 0.8 copy-start.4
  188.0 6.3 %copy-start.11 = (bf16[128,688]{0,1:T(8,128)(2,1)S(1)}, bf16[128,688]{0,1:T(8,128)(2,1)}, u32[]{:S(2)}) copy-start(bf16[128,688]{0,1:T(8,128)(2,1)} %param.34) | copy-start | bytes 528388
  188.0 6.3 %copy-start.12 = (bf16[128,688]{0,1:T(8,128)(2,1)S(1)}, bf16[128,688]{0,1:T(8,128)(2,1)}, u32[]{:S(2)}) copy-start(bf16[128,688]{0,1:T(8,128)(2,1)} %param.33) | copy-start | bytes 528388
  188.2 7.1 %copy-start.35 = (f32[384]{0:T(512)S(1)}, f32[384]{0:T(512)}, u32[]{:S(2)}) copy-start(f32[384]{0:T(512)} %param.29) | copy-start | bytes 4612
  189.6 161.7 %all-to-all-start.2 = ((bf16[16,384,128]{1,2,0:T(8,128)(2,1)}), bf16[16,384,128]{1,2,0:T(8,128)(2,1)}, u32[]{:S(2)}, u32[]{:S(2)}) async-start(bf16[16,384,128]{1,2,0:T(8,128)(2,1)} %broadcast_in_dim.26), calls=%async_computation.2 | async-start | bytes 3145728 | tf_op jit(solution)/shard_map/all_to_all | solution.py:21
  194.3 231.0 %all-gather.17.cloned.1.call-start = ((), (), s32[]{:S(2)}) async-start(), calls=%async_computation.11 | async-start | bytes 5988352 | tf_op jit(solution)/shard_map/all_gather | solution.py:12
  195.1 253.8 %all-gather.15.cloned.1.call-start = ((), (), s32[]{:S(2)}) async-start(), calls=%async_computation.10 | async-start | bytes 4718592 | tf_op jit(solution)/shard_map/all_gather | solution.py:70
  223.4 0.7 copy-start.37
  223.4 0.7 copy-start.38
  226.1 1.1 copy-start.2
  227.1 1.7 copy-start.36
  229.5 1.6 copy-start.34
  323.1 17.9 %copy-start.23 = (f32[2,384]{1,0:T(2,128)S(1)}, f32[2,384]{1,0:T(2,128)}, u32[]{:S(2)}) copy-start(f32[2,384]{1,0:T(2,128)} %slice.304) | copy-start | bytes 9220
  323.1 17.9 %copy-start.24 = (f32[2,384]{1,0:T(2,128)S(1)}, f32[2,384]{1,0:T(2,128)}, u32[]{:S(2)}) copy-start(f32[2,384]{1,0:T(2,128)} %slice.305) | copy-start | bytes 9220
  323.1 17.9 %copy-start.27 = (f32[2,384]{1,0:T(2,128)S(1)}, f32[2,384]{1,0:T(2,128)}, u32[]{:S(2)}) copy-start(f32[2,384]{1,0:T(2,128)} %slice.307) | copy-start | bytes 9220
  323.1 18.0 %copy-start.20 = (f32[4,384]{1,0:T(4,128)S(1)}, f32[4,384]{1,0:T(4,128)}, u32[]{:S(2)}) copy-start(f32[4,384]{1,0:T(4,128)} %get-tuple-element.28) | copy-start | bytes 18436
  323.1 18.7 %copy-start.21 = (f32[3,384]{1,0:T(4,128)S(1)}, f32[3,384]{1,0:T(4,128)}, u32[]{:S(2)}) copy-start(f32[3,384]{1,0:T(4,128)} %slice.296) | copy-start | bytes 13828
  323.1 18.7 %copy-start.22 = (f32[3,384]{1,0:T(4,128)S(1)}, f32[3,384]{1,0:T(4,128)}, u32[]{:S(2)}) copy-start(f32[3,384]{1,0:T(4,128)} %slice.313) | copy-start | bytes 13828
  323.1 18.7 %copy-start.32 = (f32[1,384]{1,0:T(1,128)S(1)}, f32[1,384]{1,0:T(1,128)}, u32[]{:S(2)}) copy-start(f32[1,384]{1,0:T(1,128)} %slice.345) | copy-start | bytes 4612
  323.1 18.8 %copy-start.19 = (f32[7,384]{1,0:T(8,128)S(1)}, f32[7,384]{1,0:T(8,128)}, u32[]{:S(2)}) copy-start(f32[7,384]{1,0:T(8,128)} %slice.315) | copy-start | bytes 32260
  323.2 18.8 %copy-start.31 = (f32[1,384]{1,0:T(1,128)S(1)}, f32[1,384]{1,0:T(1,128)}, u32[]{:S(2)}) copy-start(f32[1,384]{1,0:T(1,128)} %slice.344) | copy-start | bytes 4612
  324.3 17.7 %copy-start.17 = (f32[15,384]{1,0:T(8,128)S(1)}, f32[15,384]{1,0:T(8,128)}, u32[]{:S(2)}) copy-start(f32[15,384]{1,0:T(8,128)} %slice.284) | copy-start | bytes 69124
  324.3 17.7 %copy-start.18 = (f32[15,384]{1,0:T(8,128)S(1)}, f32[15,384]{1,0:T(8,128)}, u32[]{:S(2)}) copy-start(f32[15,384]{1,0:T(8,128)} %slice.317) | copy-start | bytes 69124
  324.3 17.8 %copy-start.30 = (f32[1,384]{1,0:T(1,128)S(1)}, f32[1,384]{1,0:T(1,128)}, u32[]{:S(2)}) copy-start(f32[1,384]{1,0:T(1,128)} %slice.343) | copy-start | bytes 4612
  340.4 5.2 copy-start.9
  340.4 5.3 copy-start.29
  343.7 2.1 copy-start.7
  343.7 2.1 copy-start.8
  345.5 0.7 copy-start.33
  346.3 3.4 copy-start.6
  346.6 4.4 copy-start.28
  414.2 1.0 copy-start.5
  414.2 1.3 copy-start.26
  415.2 1.3 copy-start.13
  418.5 47.7 %all-to-all-start.4 = ((bf16[16,688,128]{2,1,0:T(8,128)(2,1)}), bf16[16,688,128]{2,1,0:T(8,128)(2,1)S(1)}, u32[]{:S(2)}, u32[]{:S(2)}) async-start(bf16[16,688,128]{2,1,0:T(8,128)(2,1)} %broadcast_in_dim.27), calls=%async_computation.4 | async-start | bytes 5636096 | tf_op jit(solution)/shard_map/all_to_all | solution.py:21
  477.3 56.2 %copy-start.1 = (bf16[2,192,192]{2,1,0:T(8,128)(2,1)S(1)}, bf16[2,192,192]{2,1,0:T(8,128)(2,1)}, u32[]{:S(2)}) copy-start(bf16[2,192,192]{2,1,0:T(8,128)(2,1)} %param.27) | copy-start | bytes 442372
Sparse Core Ops, SparseCore 0:
  10.0 35.6 all-gather.6
  47.8 63.4 all-gather.8
  113.4 47.9 all-gather.12
  188.2 30.1 all-gather.10
  220.4 62.0 all-gather.16
  416.6 32.2 all-gather.14
where the time goes:
time: 544 us; the launch traced here: 540 us
  blocking collectives  162 us (30%)
  waiting for transfers between devices  144 us (26%)
  local copies, waits for them, and re-layouts  108 us (20%)
  matrix products  55.6 us (10%)
  other arithmetic  35.3 us (6%)
  starting transfers between devices  20.5 us (4%)
  between operations  14.4 us (3%)
    all_to_all x3, blocking collectives, sent_and_summed(): tiles = lax.all_to_all(cut_along(x, dim, devices), axis, 0, 0, tiled=True)  162 us
    slice x60, local copies, waits for them, and re-layouts, recurrent(): lax.associative_scan(combine, (decay_rate, drive_in), axis=0)  92.2 us
    all_gather x3, waiting for transfers between devices, sublayer(): piece = lax.all_gather(normal, 'tp', axis=0, tiled=True)  69 us
    all_gather x3, waiting for transfers between devices, in_one_piece(): lax.all_gather(both, axis, axis=dim, tiled=True)  65.6 us
    dot_general x3, matrix products, sublayer(): jnp.dot(picked, full_out, preferred_element_type=jnp.float32)  32.4 us
    dot_general x3, matrix products, sublayer(): jnp.dot(piece, full_first, preferred_element_type=jnp.float32)  20.4 us
    all_to_all x3, starting transfers between devices, copy_for_each(): return lax.all_to_all(copies, axis, split_axis=0, concat_axis=0, tiled=True)  20.1 us
    mul x8, other arithmetic, combine(): return (decay_one * decay_two, decay_two * drive_one + drive_two)  14.1 us
  transfers between devices with their start and end apart: 9, of which 5 were waited for; matrix products, arithmetic and copies ran while one was open for 34% of the time, Pallas kernels for 0%

commit v1 on v0

--- a/solution.py
+++ b/solution.py
@@ -67,7 +67,25 @@
 ):
     normal = normed(residual_activations, norm_scale_vector)
     full_first, full_second = in_one_piece((first_weight, second_weight), "fs", 0, 1)
-    piece = lax.all_gather(normal, "tp", axis=0, tiled=True)
+    a_next, shaped, main = (lax.axis_size("tp"), lax.axis_index("tp"), normal.shape[0])
+    pile = tuple(((h, (h + 1) % a_next) for h in range(a_next)))
+    frames = tuple(((h, (h - 1) % a_next) for h in range(a_next)))
+    piece = jnp.zeros((*normal.shape[:0], a_next * main, *normal.shape[1:]), normal.dtype)
+    piece = lax.dynamic_update_slice_in_dim(piece, normal, shaped * main, axis=0)
+    mid_arr = z = normal
+    res = a_next // 2
+    hop_no = 1
+    while hop_no < res + 1:
+        mid_arr = lax.ppermute(mid_arr, axis_name="tp", perm=pile)
+        piece = lax.dynamic_update_slice_in_dim(
+            piece, mid_arr, (shaped - hop_no) % a_next * main, axis=0
+        )
+        if hop_no < a_next - res:
+            z = lax.ppermute(z, axis_name="tp", perm=frames)
+            piece = lax.dynamic_update_slice_in_dim(
+                piece, z, (shaped + hop_no) % a_next * main, axis=0
+            )
+        hop_no += 1
     projected = middle(
         jnp.dot(piece, full_first, preferred_element_type=jnp.float32),
         jnp.dot(piece, full_second, preferred_element_type=jnp.float32),

time: 544 us -> 576 us (1.059)
  waiting for transfers between devices: 144 us -> 101 us
  local copies, waits for them, and re-layouts: 108 us -> 145 us
  starting transfers between devices: 20.5 us -> 42.9 us
  other arithmetic: 35.3 us -> 45.4 us
    all_gather x3 -> x0, waiting for transfers between devices: 69 us -> none  [sublayer(): piece = lax.all_gather(normal, 'tp', axis=0, tiled=True)]
    ppermute x0 -> x21, waiting for transfers between devices: none -> 41.1 us  [the longest x9 22 us: sublayer(): z = lax.ppermute(z, axis_name='tp', perm=frames)]
    dynamic_update_slice x0 -> x21, local copies, waits for them, and re-layouts: none -> 25.1 us  [the longest x12 14.3 us: sublayer(): lax.dynamic_update_slice_in_dim(piece, mid_arr, (shaped - hop_no) % a_nex...]
    ppermute x0 -> x21, starting transfers between devices: none -> 24 us  [the longest x12 18.6 us: sublayer(): mid_arr = lax.ppermute(mid_arr, axis_name='tp', perm=pile)]
    all_gather x3, waiting for transfers between devices: 65.6 us -> 45.5 us  [in_one_piece(): lax.all_gather(both, axis, axis=dim, tiled=True)]
    dot_general x0 -> x2, matrix products: none -> 15.4 us  [sublayer(): jnp.dot(piece, full_second, preferred_element_type=jnp.float32)]
    dot_general x3 -> x1, matrix products: 20.4 us -> 5.09 us  [sublayer(): jnp.dot(piece, full_first, preferred_element_type=jnp.float32)]
    pad x18, local copies, waits for them, and re-layouts: 3.85 us -> 10.2 us  [recurrent(): lax.associative_scan(combine, (decay_rate, drive_in), axis=0)]
  transfers between devices with their start and end apart: 9 -> 27, of which waited for: 5 -> 11; matrix products, arithmetic and copies ran while one was open for 34% -> 40% of each run, Pallas kernels for 0% -> 0%
where the time goes in v1:
time: 576 us; the launch traced here: 571 us
  blocking collectives  167 us (29%)
  local copies, waits for them, and re-layouts  145 us (25%)
  waiting for transfers between devices  101 us (18%)
  matrix products  56.2 us (10%)
  other arithmetic  45.4 us (8%)
  starting transfers between devices  42.9 us (7%)
  between operations  13.9 us (2%)
    all_to_all x3, blocking collectives, sent_and_summed(): tiles = lax.all_to_all(cut_along(x, dim, devices), axis, 0, 0, tiled=True)  167 us
    slice x60, local copies, waits for them, and re-layouts, recurrent(): lax.associative_scan(combine, (decay_rate, drive_in), axis=0)  90.3 us
    all_gather x3, waiting for transfers between devices, in_one_piece(): lax.all_gather(both, axis, axis=dim, tiled=True)  45.5 us
    dot_general x3, matrix products, sublayer(): jnp.dot(picked, full_out, preferred_element_type=jnp.float32)  32.9 us
    ppermute x9, waiting for transfers between devices, sublayer(): z = lax.ppermute(z, axis_name='tp', perm=frames)  22 us
    ppermute x12, waiting for transfers between devices, sublayer(): mid_arr = lax.ppermute(mid_arr, axis_name='tp', perm=pile)  19 us
    ppermute x12, starting transfers between devices, sublayer(): mid_arr = lax.ppermute(mid_arr, axis_name='tp', perm=pile)  18.6 us
    all_to_all x3, starting transfers between devices, copy_for_each(): return lax.all_to_all(copies, axis, split_axis=0, concat_axis=0, tiled=True)  18.6 us
  transfers between devices with their start and end apart: 27, of which 11 were waited for; matrix products, arithmetic and copies ran while one was open for 40% of the time, Pallas kernels for 0%

profile of v1, /device:TPU:1, one launch (start us, length us, event | category | flops | bytes accessed | tf_op | source)
XLA Modules:
  0.0 571.4 jit_solution(10298296681874629518)
XLA Ops:
  9.7 2.6 broadcast.120.clone.1
  13.5 2.6 collective-permute-start
  16.1 6.4 %collective-permute-done = bf16[128,2048]{1,0:T(8,128)(2,1)} collective-permute-done((bf16[128,2048]{1,0:T(8,128)(2,1)}, bf16[128,2048]{1,0:T(8,128)(2,1)}, u32[]{:S(2)}, u32[]{:S(2)}) %collective-permute-start) | collective-permute-done | bytes 524320 | tf_op jit(solution)/shard_map/ppermute | solution.py:79
  22.5 2.5 collective-permute-start.2
  25.0 2.0 broadcast_in_dim.10
  26.9 7.8 %all-to-all-start = ((bf16[16,688,128]{2,1,0:T(8,128)(2,1)}), bf16[16,688,128]{2,1,0:T(8,128)(2,1)S(1)}, u32[]{:S(2)}, u32[]{:S(2)}) async-start(bf16[16,688,128]{2,1,0:T(8,128)(2,1)} %broadcast_in_dim.10), calls=%async_computation | async-start | bytes 5636096 | tf_op jit(solution)/shard_map/all_to_all | solution.py:21
  50.3 2.7 collective-permute-done.5
  54.7 45.5 %all-gather.4.cloned.1.call-done = bf16[2048,1376]{0,1:T(8,128)(2,1)} async-done(((bf16[128,1376]{0,1:T(8,128)(2,1)}), bf16[2048,1376]{0,1:T(8,128)(2,1)}) %all-gather.4.cloned.1.call-update) | async-done | bytes 5636112 | tf_op jit(solution)/shard_map/all_gather | solution.py:12
  100.2 7.7 %fusion.8 = f32[1024,688]{0,1:T(8,128)} fusion(bf16[1024,2048]{1,0:T(8,128)(2,1)} %constant_dynamic-update-slice_fusion.16, bf16[2048,1376]{0,1:T(8,128)(2,1)} %all-gather.4.cloned.1.call-done), kind=kOutput, calls=%fused_computation.14 | convolution fusion | flops 2885681152 | bytes 9830400 | tf_op jit(solution)/shard_map/dot_general | solution.py:91
  107.9 11.3 %convolution_convert_fusion.2 = bf16[1024,2048]{1,0:T(8,128)(2,1)} fusion(f32[1024,688]{0,1:T(8,128)} %fusion.8, bf16[1024,2048]{1,0:T(8,128)(2,1)} %constant_dynamic-update-slice_fusion.16, bf16[2048,1376]{0,1:T(8,128)(2,1)} %all-gather.4.cloned.1.call-done, bf16[16,688,128]{2,1,0:T(8,128)(2,1)S(1)} %all-to-all-done), kind=kOutput, calls=%fused_computation.5 | convolution fusion | flops 5777686528 | bytes 16842752 | tf_op jit(solution)/shard_map/dot_general | solution.py:98
  119.2 55.2 %all_to_all.30 = bf16[8,128,2048]{2,1,0:T(8,128)(2,1)S(1)} all-to-all(bf16[8,128,2048]{2,1,0:T(8,128)(2,1)} %bitcast.50), channel_id=1, replica_groups=mesh['fs'=16,'tp'=8] {'tp'}, dimensions={0} | all-to-all | bytes 8388608 | tf_op jit(solution)/shard_map/all_to_all | solution.py:42
  176.4 2.0 copy-done.6
  180.2 6.1 %collective-permute-done.7 = bf16[128,2048]{1,0:T(8,128)(2,1)S(1)} collective-permute-done((bf16[128,2048]{1,0:T(8,128)(2,1)S(1)}, bf16[128,2048]{1,0:T(8,128)(2,1)S(1)}, u32[]{:S(2)}, u32[]{:S(2)}) %collective-permute-start.7) | collective-permute-done | bytes 524320 | tf_op jit(solution)/shard_map/ppermute | solution.py:79
  186.4 2.5 collective-permute-start.9
  190.3 4.4 all-to-all-start.2
  199.2 5.6 collective-permute-done.10
  209.1 4.7 collective-permute-done.12
  215.6 5.1 fusion.41
  228.4 3.4 fusion.32
  231.8 2.8 slice.256
  234.6 2.8 slice.257
  237.3 2.7 slice.255
  240.1 2.8 slice.259
  242.9 3.2 fusion.94
  246.0 3.1 slice.262
  249.1 3.1 slice.263
  252.2 3.1 slice.261
  255.2 3.1 slice.265
  258.3 2.4 fusion.95
  325.8 1.9 pad.68
  342.4 3.1 slice.260
  345.5 3.1 slice.325
  349.9 2.8 slice.254
  352.7 2.8 slice.327
  358.7 3.1 pad.80
  363.4 10.3 %convolution_convert_fusion = bf16[1024,2048]{1,0:T(8,128)(2,1)} fusion(bf16[384,2048]{0,1:T(8,128)(2,1)} %bitcast.12, f32[1024,384]{1,0:T(8,128)S(1)} %pad.79, f32[1024,384]{1,0:T(8,128)} %pad.80, bf16[1024,2048]{1,0:T(8,128)(2,1)} %constant_dynamic-update-slice_fusion.8, bf16[2048,768]{1,0:T(8,128)(2,1)} %all-gather.6.cloned.1.call-done), kind=kOutput, calls=%fused_computation.3 | convolution fusion | flops 3228434432 | bytes 14680064 | tf_op jit(solution)/shard_map/dot_general | solution.py:98
  373.7 57.9 %all_to_all.31 = bf16[8,128,2048]{2,1,0:T(8,128)(2,1)S(1)} all-to-all(bf16[8,128,2048]{2,1,0:T(8,128)(2,1)} %bitcast.49), channel_id=1, replica_groups=mesh['fs'=16,'tp'=8] {'tp'}, dimensions={0} | all-to-all | bytes 8388608 | tf_op jit(solution)/shard_map/all_to_all | solution.py:42
  432.9 2.6 broadcast.120
  438.4 6.4 %collective-permute-done.14 = bf16[128,2048]{1,0:T(8,128)(2,1)} collective-permute-done((bf16[128,2048]{1,0:T(8,128)(2,1)}, bf16[128,2048]{1,0:T(8,128)(2,1)}, u32[]{:S(2)}, u32[]{:S(2)}) %collective-permute-start.14) | collective-permute-done | bytes 524320 | tf_op jit(solution)/shard_map/ppermute | solution.py:79
  444.8 2.5 collective-permute-start.16
  447.3 2.0 broadcast_in_dim.27
  449.3 6.4 %all-to-all-start.4 = ((bf16[16,688,128]{2,1,0:T(8,128)(2,1)}), bf16[16,688,128]{2,1,0:T(8,128)(2,1)S(1)}, u32[]{:S(2)}, u32[]{:S(2)}) async-start(bf16[16,688,128]{2,1,0:T(8,128)(2,1)} %broadcast_in_dim.27), calls=%async_computation.4 | async-start | bytes 5636096 | tf_op jit(solution)/shard_map/all_to_all | solution.py:21
  461.2 3.6 collective-permute-done.17
  470.1 3.6 collective-permute-done.19
  475.4 7.7 %fusion.4 = f32[1024,688]{0,1:T(8,128)} fusion(bf16[1024,2048]{1,0:T(8,128)(2,1)} %constant_dynamic-update-slice_fusion, bf16[2048,1376]{0,1:T(8,128)(2,1)} %all-gather.8.cloned.1.call-done), kind=kOutput, calls=%fused_computation.10 | convolution fusion | flops 2885681152 | bytes 9830400 | tf_op jit(solution)/shard_map/dot_general | solution.py:91
  483.1 14.8 %all-to-all-done.4 = bf16[16,688,128]{2,1,0:T(8,128)(2,1)S(1)} async-done(((bf16[16,688,128]{2,1,0:T(8,128)(2,1)}), bf16[16,688,128]{2,1,0:T(8,128)(2,1)S(1)}, u32[]{:S(2)}, u32[]{:S(2)}) %all-to-all-start.4) | async-done | bytes 2818080 | tf_op jit(solution)/shard_map/all_to_all | solution.py:21
  497.9 11.3 %convolution_convert_fusion.1 = bf16[1024,2048]{1,0:T(8,128)(2,1)} fusion(f32[1024,688]{0,1:T(8,128)} %fusion.4, bf16[1024,2048]{1,0:T(8,128)(2,1)} %constant_dynamic-update-slice_fusion, bf16[2048,1376]{0,1:T(8,128)(2,1)} %all-gather.8.cloned.1.call-done, bf16[16,688,128]{2,1,0:T(8,128)(2,1)S(1)} %all-to-all-done.4), kind=kOutput, calls=%fused_computation.4 | convolution fusion | flops 5777686528 | bytes 16842752 | tf_op jit(solution)/shard_map/dot_general | solution.py:98
  509.2 54.0 %all_to_all.32 = bf16[8,128,2048]{2,1,0:T(8,128)(2,1)S(1)} all-to-all(bf16[8,128,2048]{2,1,0:T(8,128)(2,1)} %bitcast.51), channel_id=1, replica_groups=mesh['fs'=16,'tp'=8] {'tp'}, dimensions={0} | all-to-all | bytes 8388608 | tf_op jit(solution)/shard_map/all_to_all | solution.py:42
  (246 shorter events, 148.6 us)
Async XLA Ops:
  6.5 217.2 %copy-start = (bf16[2,192,192]{2,1,0:T(8,128)(2,1)S(1)}, bf16[2,192,192]{2,1,0:T(8,128)(2,1)}, u32[]{:S(2)}) copy-start(bf16[2,192,192]{2,1,0:T(8,128)(2,1)} %param.27) | copy-start | bytes 442372
  6.5 5.8 %copy-start.5 = (bf16[128,2048]{1,0:T(8,128)(2,1)S(1)}, bf16[128,2048]{1,0:T(8,128)(2,1)}, u32[]{:S(2)}) copy-start(bf16[128,2048]{1,0:T(8,128)(2,1)} %param.18) | copy-start | bytes 1572868
  6.5 5.8 %copy-start.18 = (f32[2048]{0:T(1024)S(1)}, f32[2048]{0:T(1024)}, u32[]{:S(2)}) copy-start(f32[2048]{0:T(1024)} %param.19) | copy-start | bytes 24580
  6.5 93.7 %all-gather.4.cloned.1.call-start = ((), (), s32[]{:S(2)}) async-start(), calls=%async_computation.6 | async-start | bytes 5988352 | tf_op jit(solution)/shard_map/all_gather | solution.py:12
  8.4 16.6 %copy-start.11 = (bf16[688,128]{1,0:T(8,128)(2,1)S(1)}, bf16[688,128]{1,0:T(8,128)(2,1)}, u32[]{:S(2)}) copy-start(bf16[688,128]{1,0:T(8,128)(2,1)} %param.22) | copy-start | bytes 528388
  13.5 9.0 %collective-permute-start = (bf16[128,2048]{1,0:T(8,128)(2,1)}, bf16[128,2048]{1,0:T(8,128)(2,1)}, u32[]{:S(2)}, u32[]{:S(2)}) collective-permute-start(bf16[128,2048]{1,0:T(8,128)(2,1)} %get-tuple-element.14), channel_id=1, source_target_pairs={{0,1},{1,2},{2,3},{3,4},{4,5},{5,6},{6,7},{7,0},{8,9},{9,10},{10,1... | collective-permute-start | bytes 1572872 | tf_op jit(solution)/shard_map/ppermute | solution.py:79
  16.0 18.7 %collective-permute-start.1 = (bf16[128,2048]{1,0:T(8,128)(2,1)}, bf16[128,2048]{1,0:T(8,128)(2,1)}, u32[]{:S(2)}, u32[]{:S(2)}) collective-permute-start(bf16[128,2048]{1,0:T(8,128)(2,1)} %get-tuple-element.14), channel_id=1, source_target_pairs={{0,7},{1,0},{2,1},{3,2},{4,3},{5,4},{6,5},{7,6},{8,15},{9,8},{10,9... | collective-permute-start | bytes 1572872 | tf_op jit(solution)/shard_map/ppermute | solution.py:84
  22.5 14.5 %collective-permute-start.2 = (bf16[128,2048]{1,0:T(8,128)(2,1)}, bf16[128,2048]{1,0:T(8,128)(2,1)}, u32[]{:S(2)}, u32[]{:S(2)}) collective-permute-start(bf16[128,2048]{1,0:T(8,128)(2,1)} %collective-permute-done), channel_id=1, source_target_pairs={{0,1},{1,2},{2,3},{3,4},{4,5},{5,6},{6,7},{7,0},{8,9},{9,10},{10,1... | collective-permute-start | bytes 1572872 | tf_op jit(solution)/shard_map/ppermute | solution.py:79
  26.9 81.0 %all-to-all-start = ((bf16[16,688,128]{2,1,0:T(8,128)(2,1)}), bf16[16,688,128]{2,1,0:T(8,128)(2,1)S(1)}, u32[]{:S(2)}, u32[]{:S(2)}) async-start(bf16[16,688,128]{2,1,0:T(8,128)(2,1)} %broadcast_in_dim.10), calls=%async_computation | async-start | bytes 5636096 | tf_op jit(solution)/shard_map/all_to_all | solution.py:21
  34.7 180.9 %all-gather.6.cloned.1.call-start = ((), (), s32[]{:S(2)}) async-start(), calls=%async_computation.7 | async-start | bytes 3342336 | tf_op jit(solution)/shard_map/all_gather | solution.py:12
  34.8 9.1 %collective-permute-start.3 = (bf16[128,2048]{1,0:T(8,128)(2,1)}, bf16[128,2048]{1,0:T(8,128)(2,1)}, u32[]{:S(2)}, u32[]{:S(2)}) collective-permute-start(bf16[128,2048]{1,0:T(8,128)(2,1)} %collective-permute-done.1), channel_id=1, source_target_pairs={{0,7},{1,0},{2,1},{3,2},{4,3},{5,4},{6,5},{7,6},{8,15},{9,8},{10,9... | collective-permute-start | bytes 1572872 | tf_op jit(solution)/shard_map/ppermute | solution.py:84
  37.0 9.8 %collective-permute-start.4 = (bf16[128,2048]{1,0:T(8,128)(2,1)}, bf16[128,2048]{1,0:T(8,128)(2,1)S(1)}, u32[]{:S(2)}, u32[]{:S(2)}) collective-permute-start(bf16[128,2048]{1,0:T(8,128)(2,1)} %collective-permute-done.2), channel_id=1, source_target_pairs={{0,1},{1,2},{2,3},{3,4},{4,5},{5,6},{6,7},{7,0},{8,9},{9,10},{10,1... | collective-permute-start | bytes 1572872 | tf_op jit(solution)/shard_map/ppermute | solution.py:79
  43.9 9.1 %collective-permute-start.5 = (bf16[128,2048]{1,0:T(8,128)(2,1)}, bf16[128,2048]{1,0:T(8,128)(2,1)S(1)}, u32[]{:S(2)}, u32[]{:S(2)}) collective-permute-start(bf16[128,2048]{1,0:T(8,128)(2,1)} %collective-permute-done.3), channel_id=1, source_target_pairs={{0,7},{1,0},{2,1},{3,2},{4,3},{5,4},{6,5},{7,6},{8,15},{9,8},{10,9... | collective-permute-start | bytes 1572872 | tf_op jit(solution)/shard_map/ppermute | solution.py:84
  46.8 7.1 %collective-permute-start.6 = (bf16[128,2048]{1,0:T(8,128)(2,1)S(1)}, bf16[128,2048]{1,0:T(8,128)(2,1)S(1)}, u32[]{:S(2)}, u32[]{:S(2)}) collective-permute-start(bf16[128,2048]{1,0:T(8,128)(2,1)S(1)} %collective-permute-done.4), channel_id=1, source_target_pairs={{0,1},{1,2},{2,3},{3,4},{4,5},{5,6},{6,7},{7,0},{8,9},{9,10},{10,1... | collective-permute-start | bytes 1572872 | tf_op jit(solution)/shard_map/ppermute | solution.py:79
  175.1 1.1 copy-start.19
  175.4 13.4 %copy-start.15 = (bf16[384,128]{1,0:T(8,128)(2,1)S(1)}, bf16[384,128]{1,0:T(8,128)(2,1)}, u32[]{:S(2)}) copy-start(bf16[384,128]{1,0:T(8,128)(2,1)} %param.31) | copy-start | bytes 294916
  176.2 18.7 %copy-start.12 = (bf16[128,688]{0,1:T(8,128)(2,1)S(1)}, bf16[128,688]{0,1:T(8,128)(2,1)}, u32[]{:S(2)}) copy-start(bf16[128,688]{0,1:T(8,128)(2,1)} %param.34) | copy-start | bytes 528388
  176.2 18.7 %copy-start.13 = (bf16[128,688]{0,1:T(8,128)(2,1)S(1)}, bf16[128,688]{0,1:T(8,128)(2,1)}, u32[]{:S(2)}) copy-start(bf16[128,688]{0,1:T(8,128)(2,1)} %param.33) | copy-start | bytes 528388
  176.4 2.1 copy-start.6
  178.5 18.0 %copy-start.23 = (f32[384]{0:T(512)S(1)}, f32[384]{0:T(512)}, u32[]{:S(2)}) copy-start(f32[384]{0:T(512)} %param.29) | copy-start | bytes 4612
  178.5 7.9 %collective-permute-start.7 = (bf16[128,2048]{1,0:T(8,128)(2,1)S(1)}, bf16[128,2048]{1,0:T(8,128)(2,1)S(1)}, u32[]{:S(2)}, u32[]{:S(2)}) collective-permute-start(bf16[128,2048]{1,0:T(8,128)(2,1)S(1)} %get-tuple-element.10), channel_id=1, source_target_pairs={{0,1},{1,2},{2,3},{3,4},{4,5},{5,6},{6,7},{7,0},{8,9},{9,10},{10,1... | collective-permute-start | bytes 1572872 | tf_op jit(solution)/shard_map/ppermute | solution.py:79
  180.2 15.5 %collective-permute-start.8 = (bf16[128,2048]{1,0:T(8,128)(2,1)S(1)}, bf16[128,2048]{1,0:T(8,128)(2,1)S(1)}, u32[]{:S(2)}, u32[]{:S(2)}) collective-permute-start(bf16[128,2048]{1,0:T(8,128)(2,1)S(1)} %get-tuple-element.10), channel_id=1, source_target_pairs={{0,7},{1,0},{2,1},{3,2},{4,3},{5,4},{6,5},{7,6},{8,15},{9,8},{10,9... | collective-permute-start | bytes 1572872 | tf_op jit(solution)/shard_map/ppermute | solution.py:84
  186.4 10.1 %collective-permute-start.9 = (bf16[128,2048]{1,0:T(8,128)(2,1)S(1)}, bf16[128,2048]{1,0:T(8,128)(2,1)S(1)}, u32[]{:S(2)}, u32[]{:S(2)}) collective-permute-start(bf16[128,2048]{1,0:T(8,128)(2,1)S(1)} %collective-permute-done.7), channel_id=1, source_target_pairs={{0,1},{1,2},{2,3},{3,4},{4,5},{5,6},{6,7},{7,0},{8,9},{9,10},{10,1... | collective-permute-start | bytes 1572872 | tf_op jit(solution)/shard_map/ppermute | solution.py:79
  190.3 173.0 %all-to-all-start.2 = ((bf16[16,384,128]{1,2,0:T(8,128)(2,1)}), bf16[16,384,128]{1,2,0:T(8,128)(2,1)}, u32[]{:S(2)}, u32[]{:S(2)}) async-start(bf16[16,384,128]{1,2,0:T(8,128)(2,1)} %broadcast_in_dim.26), calls=%async_computation.2 | async-start | bytes 3145728 | tf_op jit(solution)/shard_map/all_to_all | solution.py:21
  194.7 280.7 %all-gather.8.cloned.1.call-start = ((), (), s32[]{:S(2)}) async-start(), calls=%async_computation.8 | async-start | bytes 5988352 | tf_op jit(solution)/shard_map/all_gather | solution.py:12
  195.8 9.0 %collective-permute-start.10 = (bf16[128,2048]{1,0:T(8,128)(2,1)S(1)}, bf16[128,2048]{1,0:T(8,128)(2,1)S(1)}, u32[]{:S(2)}, u32[]{:S(2)}) collective-permute-start(bf16[128,2048]{1,0:T(8,128)(2,1)S(1)} %collective-permute-done.8), channel_id=1, source_target_pairs={{0,7},{1,0},{2,1},{3,2},{4,3},{5,4},{6,5},{7,6},{8,15},{9,8},{10,9... | collective-permute-start | bytes 1572872 | tf_op jit(solution)/shard_map/ppermute | solution.py:84
  196.5 10.3 %collective-permute-start.11 = (bf16[128,2048]{1,0:T(8,128)(2,1)S(1)}, bf16[128,2048]{1,0:T(8,128)(2,1)S(1)}, u32[]{:S(2)}, u32[]{:S(2)}) collective-permute-start(bf16[128,2048]{1,0:T(8,128)(2,1)S(1)} %collective-permute-done.9), channel_id=1, source_target_pairs={{0,1},{1,2},{2,3},{3,4},{4,5},{5,6},{6,7},{7,0},{8,9},{9,10},{10,1... | collective-permute-start | bytes 1572872 | tf_op jit(solution)/shard_map/ppermute | solution.py:79
  204.8 9.0 %collective-permute-start.12 = (bf16[128,2048]{1,0:T(8,128)(2,1)S(1)}, bf16[128,2048]{1,0:T(8,128)(2,1)S(1)}, u32[]{:S(2)}, u32[]{:S(2)}) collective-permute-start(bf16[128,2048]{1,0:T(8,128)(2,1)S(1)} %collective-permute-done.10), channel_id=1, source_target_pairs={{0,7},{1,0},{2,1},{3,2},{4,3},{5,4},{6,5},{7,6},{8,15},{9,8},{10,9... | collective-permute-start | bytes 1572872 | tf_op jit(solution)/shard_map/ppermute | solution.py:84
  206.8 7.9 %collective-permute-start.13 = (bf16[128,2048]{1,0:T(8,128)(2,1)S(1)}, bf16[128,2048]{1,0:T(8,128)(2,1)S(1)}, u32[]{:S(2)}, u32[]{:S(2)}) collective-permute-start(bf16[128,2048]{1,0:T(8,128)(2,1)S(1)} %collective-permute-done.11), channel_id=1, source_target_pairs={{0,1},{1,2},{2,3},{3,4},{4,5},{5,6},{6,7},{7,0},{8,9},{9,10},{10,1... | collective-permute-start | bytes 1572872 | tf_op jit(solution)/shard_map/ppermute | solution.py:79
  224.4 1.7 copy-start.24
  226.7 1.6 copy-start.22
  338.9 16.6 %copy-start.16 = (f32[16,384]{1,0:T(8,128)S(1)}, f32[16,384]{1,0:T(8,128)}, u32[]{:S(2)}) copy-start(f32[16,384]{1,0:T(8,128)} %pad_maximum_fusion.8) | copy-start | bytes 73732
  338.9 16.6 %copy-start.17 = (f32[16,384]{1,0:T(8,128)S(1)}, f32[16,384]{1,0:T(8,128)}, u32[]{:S(2)}) copy-start(f32[16,384]{1,0:T(8,128)} %add.341) | copy-start | bytes 73732
  352.7 5.1 copy-start.10
  355.6 2.4 copy-start.8
  355.6 2.4 copy-start.9
  358.5 3.3 copy-start.7
  432.6 2.9 copy-start.20
  432.9 14.4 %copy-start.14 = (bf16[688,128]{1,0:T(8,128)(2,1)S(1)}, bf16[688,128]{1,0:T(8,128)(2,1)}, u32[]{:S(2)}) copy-start(bf16[688,128]{1,0:T(8,128)(2,1)} %param.35) | copy-start | bytes 528388
  436.6 8.2 %collective-permute-start.14 = (bf16[128,2048]{1,0:T(8,128)(2,1)}, bf16[128,2048]{1,0:T(8,128)(2,1)}, u32[]{:S(2)}, u32[]{:S(2)}) collective-permute-start(bf16[128,2048]{1,0:T(8,128)(2,1)} %get-tuple-element.6), channel_id=1, source_target_pairs={{0,1},{1,2},{2,3},{3,4},{4,5},{5,6},{6,7},{7,0},{8,9},{9,10},{10,1... | collective-permute-start | bytes 1572872 | tf_op jit(solution)/shard_map/ppermute | solution.py:79
  438.4 17.3 %collective-permute-start.15 = (bf16[128,2048]{1,0:T(8,128)(2,1)}, bf16[128,2048]{1,0:T(8,128)(2,1)}, u32[]{:S(2)}, u32[]{:S(2)}) collective-permute-start(bf16[128,2048]{1,0:T(8,128)(2,1)} %get-tuple-element.6), channel_id=1, source_target_pairs={{0,7},{1,0},{2,1},{3,2},{4,3},{5,4},{6,5},{7,6},{8,15},{9,8},{10,9... | collective-permute-start | bytes 1572872 | tf_op jit(solution)/shard_map/ppermute | solution.py:84
  444.8 11.7 %collective-permute-start.16 = (bf16[128,2048]{1,0:T(8,128)(2,1)}, bf16[128,2048]{1,0:T(8,128)(2,1)}, u32[]{:S(2)}, u32[]{:S(2)}) collective-permute-start(bf16[128,2048]{1,0:T(8,128)(2,1)} %collective-permute-done.14), channel_id=1, source_target_pairs={{0,1},{1,2},{2,3},{3,4},{4,5},{5,6},{6,7},{7,0},{8,9},{9,10},{10,1... | collective-permute-start | bytes 1572872 | tf_op jit(solution)/shard_map/ppermute | solution.py:79
  449.3 48.7 %all-to-all-start.4 = ((bf16[16,688,128]{2,1,0:T(8,128)(2,1)}), bf16[16,688,128]{2,1,0:T(8,128)(2,1)S(1)}, u32[]{:S(2)}, u32[]{:S(2)}) async-start(bf16[16,688,128]{2,1,0:T(8,128)(2,1)} %broadcast_in_dim.27), calls=%async_computation.4 | async-start | bytes 5636096 | tf_op jit(solution)/shard_map/all_to_all | solution.py:21
  455.7 9.1 %collective-permute-start.17 = (bf16[128,2048]{1,0:T(8,128)(2,1)}, bf16[128,2048]{1,0:T(8,128)(2,1)S(1)}, u32[]{:S(2)}, u32[]{:S(2)}) collective-permute-start(bf16[128,2048]{1,0:T(8,128)(2,1)} %collective-permute-done.15), channel_id=1, source_target_pairs={{0,7},{1,0},{2,1},{3,2},{4,3},{5,4},{6,5},{7,6},{8,15},{9,8},{10,9... | collective-permute-start | bytes 1572872 | tf_op jit(solution)/shard_map/ppermute | solution.py:84
  456.5 11.6 %collective-permute-start.18 = (bf16[128,2048]{1,0:T(8,128)(2,1)}, bf16[128,2048]{1,0:T(8,128)(2,1)S(1)}, u32[]{:S(2)}, u32[]{:S(2)}) collective-permute-start(bf16[128,2048]{1,0:T(8,128)(2,1)} %collective-permute-done.16), channel_id=1, source_target_pairs={{0,1},{1,2},{2,3},{3,4},{4,5},{5,6},{6,7},{7,0},{8,9},{9,10},{10,1... | collective-permute-start | bytes 1572872 | tf_op jit(solution)/shard_map/ppermute | solution.py:79
  464.8 8.9 %collective-permute-start.19 = (bf16[128,2048]{1,0:T(8,128)(2,1)S(1)}, bf16[128,2048]{1,0:T(8,128)(2,1)S(1)}, u32[]{:S(2)}, u32[]{:S(2)}) collective-permute-start(bf16[128,2048]{1,0:T(8,128)(2,1)S(1)} %collective-permute-done.17), channel_id=1, source_target_pairs={{0,7},{1,0},{2,1},{3,2},{4,3},{5,4},{6,5},{7,6},{8,15},{9,8},{10,9... | collective-permute-start | bytes 1572872 | tf_op jit(solution)/shard_map/ppermute | solution.py:84
  468.1 6.5 %collective-permute-start.20 = (bf16[128,2048]{1,0:T(8,128)(2,1)S(1)}, bf16[128,2048]{1,0:T(8,128)(2,1)S(1)}, u32[]{:S(2)}, u32[]{:S(2)}) collective-permute-start(bf16[128,2048]{1,0:T(8,128)(2,1)S(1)} %collective-permute-done.18), channel_id=1, source_target_pairs={{0,1},{1,2},{2,3},{3,4},{4,5},{5,6},{6,7},{7,0},{8,9},{9,10},{10,1... | collective-permute-start | bytes 1572872 | tf_op jit(solution)/shard_map/ppermute | solution.py:79
  509.2 55.6 %copy-start.1 = (bf16[2,192,192]{2,1,0:T(8,128)(2,1)S(1)}, bf16[2,192,192]{2,1,0:T(8,128)(2,1)}, u32[]{:S(2)}) copy-start(bf16[2,192,192]{2,1,0:T(8,128)(2,1)} %param.27) | copy-start | bytes 442372
  (6 other events, 5.0 us)
Sparse Core Ops, SparseCore 0:
  9.4 90.7 all-gather.3
  102.4 47.7 all-gather.5
  197.7 66.1 all-gather.7
